TPU v7x, 512 devices: a whole 4x8x8 slice. The times are simulated.
512 devices in a mesh: fs: 64 (over z, y), tp: 8 (over x, core).
Axes of the slice: x: 4, y: 8, z: 8, core: 2. Of those that a mesh axis runs over, the one named last changes fastest.
Arguments:
- x_late: bfloat16 [16384, 2048], P('fs'), may hold values from -6 to 6
- x_early: bfloat16 [16384, 2048], P('fs'), may hold values from -6 to 6
- cotangent: bfloat16 [16384, 2048], P('fs'), may hold values from -16 to 16
- w_gate: bfloat16 [2048, 4096], P('fs', 'tp'), may hold values from -0.125 to 0.125
- w_up: bfloat16 [2048, 4096], P('fs', 'tp'), may hold values from -0.125 to 0.125
- w_down: bfloat16 [4096, 2048], P('tp', 'fs'), may hold values from -0.09375 to 0.09375
- conv_taps: float32 [3, 4096], replicated, may hold values from -3 to 3
- conv_bias: float32 [4096], replicated, may hold values from -3 to 3
- grad_down: float32 [4096, 2048], P('tp', 'fs'), may hold values from -60 to 60
Outputs:
- y_late: bfloat16 [16384, 2048], P('fs')
- dx_early: bfloat16 [16384, 2048], P('fs')
- grad_down_out: float32 [4096, 2048], P('tp', 'fs')
All inputs are finite; a program needn't handle non-finite values.
Results may differ from a plain program's by a relative error of at most 0.017.
Values may be sent and summed in bfloat16 or wider, within the bound.
No kernel may reach another device: no remote copies, remote signals or barrier semaphores. Data moves between devices by JAX's collectives and lax.ppermute only.
A program may use at most 128 MiB of HBM per device.

v0:
```python
import jax
import jax.numpy as jnp
from jax import lax
from jax.sharding import Mesh
from jax.sharding import PartitionSpec as P

FS = ("fs_0", "fs_1")


def total_of_pieces(value, axis):
    pieces = lax.all_gather(value, axis).astype(jnp.float32)
    return pieces.sum(axis=0)


def in_blocks(value, dim, peers):
    lengths = value.shape
    pieces = value.reshape(*lengths[:dim], peers, lengths[dim] // peers, *lengths[dim + 1 :])
    return jnp.moveaxis(pieces, dim, 0)


def sent_and_summed(value, axis, dim):
    pieces = in_blocks(value, dim, lax.axis_size(axis))
    arrived = lax.all_to_all(pieces, axis, split_axis=0, concat_axis=0, tiled=True)
    return arrived.astype(jnp.float32).sum(axis=0)


def in_one_piece(arrays, axis, dim, along):
    both = jnp.concatenate(arrays, axis=along)
    out, at, done = (lax.all_gather(both, axis, axis=dim, tiled=True), 0, [])
    for a in arrays:
        done.append(lax.slice_in_dim(out, at, at + a.shape[along], axis=along))
        at += a.shape[along]
    return tuple(done)


def laid_out(pieces, dim):
    lengths = list(pieces.shape[1:])
    lengths[dim] *= pieces.shape[0]
    return jnp.moveaxis(pieces, 0, dim).reshape(lengths)


def stacked_from(value, axes, turns):
    pieces = value
    for k in turns:
        pieces = lax.all_gather(pieces, axes[k])
    done = turns[::-1]
    back = [done.index(k) for k in range(len(axes))]
    pieces = pieces.transpose(*back, *range(len(axes), pieces.ndim))
    return pieces.reshape(-1, *value.shape)


def gathered_by_axis(value, axes, turns, dim):
    return laid_out(stacked_from(value, axes, turns), dim)


def shift_later(field, steps):
    pad = jnp.zeros((steps, field.shape[1]), jnp.float32)
    return jnp.concatenate([pad, field[: field.shape[0] - steps]], axis=0)


def shift_earlier(field, steps):
    pad = jnp.zeros((steps, field.shape[1]), jnp.float32)
    return jnp.concatenate([field[steps:], pad], axis=0)


def contract_last(left, right):
    return lax.dot_general(
        left, right, (((1,), (1,)), ((), ())), preferred_element_type=jnp.float32
    )


def hidden_parts(inputs, gate_full, up_full, taps, bias):
    gate = (
        jnp.dot(inputs, gate_full, preferred_element_type=jnp.float32)
        .astype(jnp.bfloat16)
        .astype(jnp.float32)
    )
    up = jnp.dot(inputs, up_full, preferred_element_type=jnp.float32)
    conv = bias + taps[2] * gate + taps[1] * shift_later(gate, 1) + taps[0] * shift_later(gate, 2)
    act = jax.nn.silu(conv)
    hidden = (act * up).astype(jnp.bfloat16)
    return (conv, act, up, hidden)


def forward_pass(x_late, gate_full, up_full, down_full, taps, bias):
    conv, act, up, hidden = hidden_parts(x_late, gate_full, up_full, taps, bias)
    partial_value = jnp.dot(hidden, down_full, preferred_element_type=jnp.float32)
    return (
        total_of_pieces(partial_value.astype(jnp.bfloat16), "tp")
        .astype(jnp.float32)
        .astype(jnp.bfloat16)
    )


def backward_pass(x_early, cotangent, gate_full, up_full, down_full, taps, bias, grad_down):
    conv, act, up, hidden = hidden_parts(x_early, gate_full, up_full, taps, bias)
    dhidden = contract_last(cotangent, down_full)
    summed = sent_and_summed(
        lax.dot_general(
            cotangent, hidden, (((0,), (0,)), ((), ())), preferred_element_type=jnp.float32
        ).astype(jnp.bfloat16),
        FS,
        0,
    )
    grad_down_out = grad_down + summed.T
    dup = (dhidden * act).astype(jnp.bfloat16)
    sig = jax.nn.sigmoid(conv)
    dconv = dhidden * up * sig * (1.0 + conv * (1.0 - sig))
    dgate = taps[2] * dconv + taps[1] * shift_earlier(dconv, 1) + taps[0] * shift_earlier(dconv, 2)
    dgate = dgate.astype(jnp.bfloat16)
    partial_value = contract_last(dup, up_full) + contract_last(dgate, gate_full)
    dx_early = (
        total_of_pieces(partial_value.astype(jnp.bfloat16), "tp")
        .astype(jnp.float32)
        .astype(jnp.bfloat16)
    )
    return (dx_early, grad_down_out)


def shards(x_late, x_early, cotangent, w_gate, w_up, w_down, conv_taps, conv_bias, grad_down):
    width = w_gate.shape[1]
    offset = lax.axis_index("tp") * width
    taps = lax.dynamic_slice_in_dim(conv_taps, offset, width, 1)
    bias = lax.dynamic_slice_in_dim(conv_bias, offset, width, 0)
    gate_full, up_full = in_one_piece((w_gate, w_up), FS, 0, 1)
    down_full = gathered_by_axis(w_down, FS, (0, 1), 1)
    y_late = forward_pass(x_late, gate_full, up_full, down_full, taps, bias)
    dx_early, grad_down_out = backward_pass(
        x_early, cotangent, gate_full, up_full, down_full, taps, bias, grad_down
    )
    return (y_late, dx_early, grad_down_out)


def solution(mesh):
    torus = Mesh(mesh.devices.reshape(8, 8, mesh.shape["tp"]), ("fs_0", "fs_1", "tp"))
    return jax.shard_map(
        shards,
        mesh=torus,
        in_specs=(
            P(FS, None),
            P(FS, None),
            P(FS, None),
            P(FS, "tp"),
            P(FS, "tp"),
            P("tp", FS),
            P(),
            P(),
            P("tp", FS),
        ),
        out_specs=(P(FS, None), P(FS, None), P("tp", FS)),
        check_vma=False,
    )
```

profile of v0, /device:TPU:1, one launch (start us, length us, event | category | flops | bytes accessed | tf_op | source)
XLA Modules:
  0.0 302.9 jit_solution(3665544299744078919)
XLA Ops:
  7.2 0.0 copy-start
  7.2 0.0 all-gather.11.cloned.1.call-start
  7.2 26.3 %all-gather = bf16[4096,32]{0,1:T(8,128)(2,1)S(1)} all-gather(bf16[512,32]{0,1:T(8,128)(2,1)} %param.14), channel_id=2, replica_groups=mesh['fs_0'=8,'fs_1'=8,'tp'=8] {'fs_0'}, dimensions={0}, use_global_device_ids=true | all-gather | bytes 294912 | tf_op jit(solution)/shard_map/all_gather | solution.py:45
  33.5 0.8 copy.28
  34.3 0.0 all-gather.11.cloned.1.call-update
  34.3 0.0 all-gather.9.cloned.1.call-start
  34.4 1.4 pad_maximum_fusion
  35.8 0.0 all-gather.9.cloned.1.call-update
  35.8 0.0 all-gather.13.cloned.1.call-start
  35.9 0.8 dynamic_slice.6
  36.6 0.9 fusion.74
  37.5 40.6 %all-gather.11.cloned.1.call-done = bf16[64,512,32]{1,0,2:T(8,128)(2,1)} async-done(((bf16[8,512,32]{1,0,2:T(8,128)(2,1)}), bf16[64,512,32]{1,0,2:T(8,128)(2,1)}) %all-gather.11.cloned.1.call-update) | async-done | bytes 2097168 | tf_op jit(solution)/shard_map/all_gather | solution.py:45
  78.1 2.8 copy.22
  80.9 86.5 %all-gather.9.cloned.1.call-done = bf16[2048,1024]{1,0:T(8,128)(2,1)} async-done(((bf16[32,1024]{1,0:T(8,128)(2,1)}), bf16[2048,1024]{1,0:T(8,128)(2,1)}) %all-gather.9.cloned.1.call-update) | async-done | bytes 4194320 | tf_op jit(solution)/shard_map/all_gather | solution.py:29
  167.4 3.4 %fusion.40 = f32[256,512]{0,1:T(8,128)} fusion(bf16[256,2048]{1,0:T(8,128)(2,1)} %param.9, bf16[2048,1024]{1,0:T(8,128)(2,1)} %all-gather.9.cloned.1.call-done), kind=kOutput, calls=%fused_computation.26 | convolution fusion | flops 537133056 | bytes 3670016 | tf_op jit(solution)/shard_map/dot_general | solution.py:74
  170.8 5.8 %convolution_convert_fusion.1 = bf16[256,2048]{1,0:T(8,128)(2,1)} fusion(bf16[512,2048]{0,1:T(8,128)(2,1)S(1)} %bitcast.52, bf16[256,2048]{1,0:T(8,128)(2,1)} %param.9, bf16[2048,1024]{1,0:T(8,128)(2,1)} %all-gather.9.cloned.1.call-done, f32[254,512]{0,1:T(8,128)} %bitcast.67, f32[255,512]{0,1:T(8,128)} %bitcast.68, f32[256,512]{0,1:T(8,128)} %fusion.40, ...), kind=kOutput, calls=%fused_computation.5 | convolution fusion | flops 1075838976 | bytes 7872512 | tf_op jit(solution)/shard_map/dot_general | solution.py:87
  176.7 0.0 all-gather.13.cloned.1.call-update
  176.7 0.0 all-gather.15.cloned.1.call-start
  176.7 0.0 copy-start.1
  176.7 2.8 fusion.34
  179.5 0.3 copy-done.1
  179.9 2.0 fusion.19
  181.8 0.0 copy-start.3
  181.9 0.0 copy-done
  181.9 1.2 add_multiply_fusion
  183.1 0.0 copy-done.3
  183.1 0.0 copy-start.5
  183.1 0.2 slice.57
  183.3 0.2 slice.56
  183.6 0.8 fusion.4
  184.3 0.0 copy-done.5
  184.4 0.0 copy-start.4
  184.4 2.0 fusion.1
  186.4 0.0 all-gather.15.cloned.1.call-update
  186.4 0.0 copy-done.4
  186.4 3.1 %fusion = bf16[2048,512]{0,1:T(8,128)(2,1)} fusion(bf16[256,2048]{1,0:T(8,128)(2,1)S(1)} %copy-done, f32[256,512]{0,1:T(8,128)S(1)} %copy-done.4, f32[256,512]{0,1:T(8,128)} %copy-done.5), kind=kOutput, calls=%fused_computation.2 | convolution fusion | flops 538705920 | bytes 4194304 | tf_op jit(solution)/shard_map/dot_general | solution.py:99
  189.6 2.9 copy.25
  192.5 52.6 %all_to_all.5 = bf16[64,32,512]{2,1,0:T(8,128)(2,1)S(1)} all-to-all(bf16[64,32,512]{2,1,0:T(8,128)(2,1)S(1)} %bitcast.50), channel_id=1, replica_groups=mesh['fs_0'=8,'fs_1'=8,'tp'=8] {'fs_0','fs_1'}, dimensions={0} | all-to-all | bytes 4194304 | tf_op jit(solution)/shard_map/all_to_all | solution.py:23
  245.1 0.0 copy-start.2
  245.1 0.3 convert_reduce_fusion
  245.4 0.5 copy-done.2
  245.9 0.6 bitcast_add_fusion
  246.6 0.0 all-gather.13.cloned.1.call-done
  246.6 6.8 %reduce_sum.33 = bf16[256,2048]{1,0:T(8,128)(2,1)} reduce(bf16[8,256,2048]{2,1,0:T(8,128)(2,1)} %bitcast.48, bf16[]{:T(256)} %constant.21.clone.1), dimensions={0}, to_apply=%region_0.1 | reduce | flops 3670016 | bytes 9437186 | tf_op jit(solution)/shard_map/reduce_sum | solution.py:12
  253.4 36.5 %all-gather.15.cloned.1.call-done = bf16[2048,2048]{1,0:T(8,128)(2,1)} async-done(((bf16[256,2048]{1,0:T(8,128)(2,1)}), bf16[2048,2048]{1,0:T(8,128)(2,1)}) %all-gather.15.cloned.1.call-update) | async-done | bytes 8388624 | tf_op jit(solution)/shard_map/all_gather | solution.py:11
  289.9 6.4 %reduce_sum.34 = bf16[256,2048]{1,0:T(8,128)(2,1)} reduce(bf16[8,256,2048]{2,1,0:T(8,128)(2,1)} %bitcast.49, bf16[]{:T(256)} %constant.21.clone.1), dimensions={0}, to_apply=%region_1.2 | reduce | flops 3670016 | bytes 9437186 | tf_op jit(solution)/shard_map/reduce_sum | solution.py:12
Async XLA Ops:
  7.2 174.7 %copy-start = (bf16[256,2048]{1,0:T(8,128)(2,1)S(1)}, bf16[256,2048]{1,0:T(8,128)(2,1)}, u32[]{:S(2)}) copy-start(bf16[256,2048]{1,0:T(8,128)(2,1)} %param.11) | copy-start | bytes 3145732
  7.2 71.0 %all-gather.11.cloned.1.call-start = ((), (), s32[]{:S(2)}) async-start(), calls=%async_computation.2 | async-start | bytes 2359296 | tf_op jit(solution)/shard_map/all_gather | solution.py:45
  34.3 133.1 %all-gather.9.cloned.1.call-start = ((), (), s32[]{:S(2)}) async-start(), calls=%async_computation.1 | async-start | bytes 4259840 | tf_op jit(solution)/shard_map/all_gather | solution.py:29
  35.8 210.8 %all-gather.13.cloned.1.call-start = ((), (), s32[]{:S(2)}) async-start(), calls=%async_computation.3 | async-start | bytes 9437184 | tf_op jit(solution)/shard_map/all_gather | solution.py:11
  176.7 113.3 %all-gather.15.cloned.1.call-start = ((), (), s32[]{:S(2)}) async-start(), calls=%async_computation.4 | async-start | bytes 9437184 | tf_op jit(solution)/shard_map/all_gather | solution.py:11
  176.7 3.1 %copy-start.1 = (bf16[2048,1024]{1,0:T(8,128)(2,1)S(1)}, bf16[2048,1024]{1,0:T(8,128)(2,1)}, u32[]{:S(2)}) copy-start(bf16[2048,1024]{1,0:T(8,128)(2,1)} %all-gather.9.cloned.1.call-done) | copy-start | bytes 12582916
  181.8 1.3 copy-start.3
  183.1 1.2 copy-start.5
  184.4 2.1 copy-start.4
  245.1 0.8 copy-start.2
Sparse Core Ops, SparseCore 0:
  34.4 43.6 all-gather.10
  81.8 85.5 all-gather.8
  176.8 55.8 all-gather.12
  234.7 55.1 all-gather.14
where the time goes:
time: 303 us
  waiting for transfers between devices  164 us (54%)
  blocking collectives  78.9 us (26%)
  matrix products  21.2 us (7%)
  other arithmetic  15.6 us (5%)
  between operations  13.9 us (5%)
  local copies, waits for them, and re-layouts  9.37 us (3%)
    all_gather x1, waiting for transfers between devices, in_one_piece(): out, at, done = (lax.all_gather(both, axis, axis=dim, tiled=True), 0, [])  86.5 us
    all_to_all x1, blocking collectives, sent_and_summed(): lax.all_to_all(pieces, axis, split_axis=0, concat_axis=0, tiled=True)  52.6 us
    all_gather x1, waiting for transfers between devices, stacked_from(): pieces = lax.all_gather(pieces, axes[k])  40.6 us
    all_gather x2, waiting for transfers between devices, total_of_pieces(): pieces = lax.all_gather(value, axis).astype(jnp.float32)  36.5 us
    all_gather x1, blocking collectives, stacked_from(): pieces = lax.all_gather(pieces, axes[k])  26.3 us
    reduce_sum x2, other arithmetic, total_of_pieces(): return pieces.sum(axis=0)  13.2 us
    dot_general x2, matrix products, hidden_parts(): jnp.dot(inputs, gate_full, preferred_element_type=jnp.float32)  6.18 us
  transfers between devices with their start and end apart: 4, of which 3 were waited for; matrix products, arithmetic and copies ran while one was open for 10% of the time, Pallas kernels for 0%

commit v1 on v0

v1 whole, which is shorter than its diff:
```python
import jax
import jax.numpy as jnp
from jax import lax
from jax.experimental import pallas as pl
from jax.experimental.pallas import tpu as pltpu
from jax.sharding import Mesh
from jax.sharding import PartitionSpec as P

AXES = ("z", "y", "x", "c")
FS = ("z", "y")
TP = ("x", "c")
NZ, NY, NX, NC = 8, 8, 4, 2
UNITS = 512
TOK = 256
WIDTH = 2048


def place(z, y, x, c):
    return ((z * NY + y) * NX + x) * NC + c


def split_groups(core_along_y):
    groups = []
    for x in range(NX):
        for k in range(8):
            groups.append([place(k, y, x, core_along_y) for y in range(NY)])
            groups.append([place(z, k, x, 1 - core_along_y) for z in range(NZ)])
    return groups


FIRST = split_groups(0)
SECOND = split_groups(1)


def contract_last(left, right):
    return lax.dot_general(
        left, right, (((1,), (1,)), ((), ())), preferred_element_type=jnp.float32
    )


def shift_later(field, steps):
    row = lax.broadcasted_iota(jnp.int32, field.shape, 0)
    return jnp.where(row >= steps, pltpu.roll(field, steps, 0), 0.0)


def shift_earlier(field, steps):
    rows = field.shape[0]
    row = lax.broadcasted_iota(jnp.int32, field.shape, 0)
    return jnp.where(row < rows - steps, pltpu.roll(field, rows - steps, 0), 0.0)


def layer_kernel(
    stride_ref, xl_ref, xe_ref, cot_ref, cot_t_ref, taps_ref, bias_ref, w_hbm,
    y_ref, dx_ref, grad_ref, w_ref, sems,
):
    outer = stride_ref[0]
    inner = stride_ref[1]

    def copy(p, j):
        at = pl.multiple_of((p * outer + j * inner) * 32, 32)
        return pltpu.make_async_copy(w_hbm.at[p, j], w_ref.at[pl.ds(at, 32)], sems.at[p, j])

    for p in range(8):
        for j in range(8):
            copy(p, j).start()
    t0, t1, t2 = taps_ref[0:1, :], taps_ref[1:2, :], taps_ref[2:3, :]
    bias = bias_ref[0:1, :]
    for p in range(8):
        for j in range(8):
            copy(p, j).wait()
    w_gate = w_ref[:, 0:UNITS]
    w_up = w_ref[:, UNITS : 2 * UNITS]
    w_down = w_ref[:, 2 * UNITS : 3 * UNITS]

    def hidden_parts(x):
        gate = jnp.dot(x, w_gate, preferred_element_type=jnp.float32)
        gate = gate.astype(jnp.bfloat16).astype(jnp.float32)
        up = jnp.dot(x, w_up, preferred_element_type=jnp.float32)
        conv = bias + t2 * gate + t1 * shift_later(gate, 1) + t0 * shift_later(gate, 2)
        sig = 1.0 / (1.0 + jnp.exp(-conv))
        act = conv * sig
        return conv, sig, act, up, (act * up).astype(jnp.bfloat16)

    conv, sig, act, up, hidden = hidden_parts(xe_ref[...])
    for k in range(8):
        part = jnp.dot(
            cot_t_ref[k * 256 : (k + 1) * 256, :], hidden, preferred_element_type=jnp.float32
        ).astype(jnp.bfloat16)
        for j in range(8):
            at = pl.multiple_of((k * outer + j * inner) * 32, 32)
            grad_ref[pl.ds(at, 32), :] = part[j * 32 : (j + 1) * 32, :]
    dhidden = jnp.dot(cot_ref[...], w_down, preferred_element_type=jnp.float32)
    dup = (dhidden * act).astype(jnp.bfloat16)
    dconv = dhidden * up * sig * (1.0 + conv * (1.0 - sig))
    dgate = t2 * dconv + t1 * shift_earlier(dconv, 1) + t0 * shift_earlier(dconv, 2)
    dgate = dgate.astype(jnp.bfloat16)
    dx_ref[...] = (contract_last(dup, w_up) + contract_last(dgate, w_gate)).astype(jnp.bfloat16)
    late = hidden_parts(xl_ref[...])[4]
    y_ref[...] = contract_last(late, w_down).astype(jnp.bfloat16)


def layer(strides, x_late, x_early, cot, cot_t, taps, bias, w):
    vmem = pl.BlockSpec(memory_space=pltpu.VMEM)
    return pl.pallas_call(
        layer_kernel,
        out_shape=(
            jax.ShapeDtypeStruct((TOK, WIDTH), jnp.bfloat16),
            jax.ShapeDtypeStruct((TOK, WIDTH), jnp.bfloat16),
            jax.ShapeDtypeStruct((WIDTH, UNITS), jnp.bfloat16),
        ),
        in_specs=[pl.BlockSpec(memory_space=pltpu.SMEM)] + [vmem] * 6
        + [pl.BlockSpec(memory_space=pl.ANY)],
        out_specs=(vmem, vmem, vmem),
        scratch_shapes=[
            pltpu.VMEM((WIDTH, 3 * UNITS), jnp.bfloat16),
            pltpu.SemaphoreType.DMA((8, 8)),
        ],
        compiler_params=pltpu.CompilerParams(vmem_limit_bytes=48 * 1024 * 1024),
        name="layer",
    )(strides, x_late, x_early, cot, cot_t, taps, bias, w)


def exchanged(value):
    return lax.ppermute(value, "c", [(0, 1), (1, 0)])


def f32_sum(pieces):
    return pieces.astype(jnp.float32).sum(axis=0).astype(jnp.bfloat16)


def shards(x_late, x_early, cotangent, w_gate, w_up, w_down, conv_taps, conv_bias, grad_down):
    core = lax.axis_index("c")
    offset = lax.axis_index(TP) * UNITS
    taps = lax.dynamic_slice_in_dim(conv_taps, offset, UNITS, 1)
    bias = lax.dynamic_slice_in_dim(conv_bias, offset, UNITS, 0)[None]
    mine = jnp.concatenate([w_gate, w_up, w_down.T], axis=1)
    near = lax.all_to_all(
        jnp.broadcast_to(mine[None], (8,) + mine.shape), AXES, 0, 0,
        tiled=True, axis_index_groups=FIRST,
    )
    w = lax.all_gather(near, AXES, axis_index_groups=SECOND)
    strides = jnp.where(core == 0, jnp.array([8, 1]), jnp.array([1, 8])).astype(jnp.int32)
    y_part, dx_part, grad_part = layer(
        strides, x_late, x_early, cotangent, cotangent.T, taps, bias, w
    )

    grad = lax.all_to_all(
        grad_part.reshape(8, 256, UNITS), AXES, 0, 0, tiled=True, axis_index_groups=SECOND
    )
    grad = f32_sum(grad).reshape(8, 32, UNITS)
    grad = lax.all_to_all(grad, AXES, 0, 0, tiled=True, axis_index_groups=FIRST)
    grad_down_out = grad_down + grad.astype(jnp.float32).sum(axis=0).T

    halves = jnp.stack([y_part.reshape(2, 128, WIDTH), dx_part.reshape(2, 128, WIDTH)], axis=1)
    keep = lax.dynamic_index_in_dim(halves, core, 0, keepdims=False)
    give = lax.dynamic_index_in_dim(halves, 1 - core, 0, keepdims=False)
    chip = (keep.astype(jnp.float32) + exchanged(give).astype(jnp.float32)).astype(jnp.bfloat16)
    pieces = chip.reshape(2, NX, 32, WIDTH).swapaxes(0, 1)
    total = f32_sum(lax.all_to_all(pieces, "x", 0, 0, tiled=True))
    total = lax.all_to_all(
        jnp.broadcast_to(total[None], (NX, 2, 32, WIDTH)), "x", 0, 0, tiled=True
    )
    total = total.swapaxes(0, 1).reshape(2, 128, WIDTH)
    other = exchanged(total)
    first = jnp.where(core == 0, total, other)
    second = jnp.where(core == 0, other, total)
    y_late = jnp.concatenate([first[0], second[0]], axis=0)
    dx_early = jnp.concatenate([first[1], second[1]], axis=0)
    return (y_late, dx_early, grad_down_out)


def solution(mesh):
    torus = Mesh(mesh.devices.reshape(NZ, NY, NX, NC), AXES)
    return jax.shard_map(
        shards,
        mesh=torus,
        in_specs=(
            P(FS, None),
            P(FS, None),
            P(FS, None),
            P(FS, TP),
            P(FS, TP),
            P(TP, FS),
            P(),
            P(),
            P(TP, FS),
        ),
        out_specs=(P(FS, None), P(FS, None), P(TP, FS)),
        check_vma=False,
    )
```

time: 303 us -> 196 us (0.65); the launches traced: 303 us -> 192 us
  waiting for transfers between devices: 164 us -> 75.3 us
  matrix products: 21.2 us -> 0 us
  blocking collectives: 78.9 us -> 60.3 us
  starting transfers between devices: 0.16 us -> 18.3 us
  Pallas kernels: 0 us -> 10.4 us
  other arithmetic: 15.6 us -> 7.73 us
  local copies, waits for them, and re-layouts: 9.37 us -> 6.27 us
    all_gather x4 -> x1, waiting for transfers between devices: 164 us -> 43.1 us  [shards(): w = lax.all_gather(near, AXES, axis_index_groups=SECOND)]
    all_to_all x0 -> x2, waiting for transfers between devices: none -> 29.7 us  [the longest x1 24 us: shards(): lax.all_to_all(grad_part.reshape(8, 256, UNITS), AXES, 0, 0, tiled=True,...]
    all_gather x1 -> x0, blocking collectives: 26.3 us -> none  [stacked_from(): pieces = lax.all_gather(pieces, axes[k])]
    dot_general x8 -> x0, matrix products: 21.2 us -> none  [the longest x2 6.18 us: hidden_parts(): jnp.dot(inputs, gate_full, preferred_element_type=jnp.float32)]
    reduce_sum x3, other arithmetic: 13.6 us -> 1.29 us  [the longest x2 1.25 us: f32_sum(): return pieces.astype(jnp.float32).sum(axis=0).astype(jnp.bfloat16)]
    pallas_call x0 -> x1, Pallas kernels: none -> 10.4 us  [layer(): pl.pallas_call(layer_kernel, out_shape=(jax.ShapeDtypeStruct((TOK, WIDTH)...]
    all_to_all x0 -> x2, starting transfers between devices: none -> 10.3 us  [the longest x1 6.46 us: shards(): lax.all_to_all(grad_part.reshape(8, 256, UNITS), AXES, 0, 0, tiled=True,...]
    ppermute x0 -> x2, starting transfers between devices: none -> 8 us  [exchanged(): return lax.ppermute(value, 'c', [(0, 1), (1, 0)])]
  transfers between devices with their start and end apart: 4 -> 5, of which waited for: 3 -> 4; matrix products, arithmetic and copies ran while one was open for 10% -> 4% of each run, Pallas kernels for 0% -> 0%
where the time goes in v1:
time: 196 us; the launch traced here: 192 us
  waiting for transfers between devices  75.3 us (38%)
  blocking collectives  60.3 us (31%)
  starting transfers between devices  18.3 us (9%)
  between operations  14.2 us (7%)
  Pallas kernels  10.4 us (5%)
  other arithmetic  7.73 us (4%)
  local copies, waits for them, and re-layouts  6.27 us (3%)
    all_gather x1, waiting for transfers between devices, shards(): w = lax.all_gather(near, AXES, axis_index_groups=SECOND)  43.1 us
    all_to_all x1, blocking collectives, shards(): lax.all_to_all(jnp.broadcast_to(mine[None], (8,) + mine.shape), AXES, 0,...  25.7 us
    all_to_all x1, waiting for transfers between devices, shards(): lax.all_to_all(grad_part.reshape(8, 256, UNITS), AXES, 0, 0, tiled=True,...  24 us
    all_to_all x1, blocking collectives, shards(): total = f32_sum(lax.all_to_all(pieces, 'x', 0, 0, tiled=True))  18 us
    all_to_all x1, blocking collectives, shards(): lax.all_to_all(jnp.broadcast_to(total[None], (NX, 2, 32, WIDTH)), 'x', 0,...  16.5 us
    pallas_call x1, Pallas kernels, layer(): pl.pallas_call(layer_kernel, out_shape=(jax.ShapeDtypeStruct((TOK, WIDTH)...  10.4 us
    ppermute x2, starting transfers between devices, exchanged(): return lax.ppermute(value, 'c', [(0, 1), (1, 0)])  8 us
    all_to_all x1, starting transfers between devices, shards(): lax.all_to_all(grad_part.reshape(8, 256, UNITS), AXES, 0, 0, tiled=True,...  6.46 us
  transfers between devices with their start and end apart: 5, of which 4 were waited for; matrix products, arithmetic and copies ran while one was open for 4% of the time, Pallas kernels for 0%

profile of v1, /device:TPU:1, one launch (start us, length us, event | category | flops | bytes accessed | tf_op | source)
XLA Modules:
  0.0 192.4 jit_solution(9151423594448669590)
XLA Ops:
  7.2 0.0 copy-start
  7.2 0.0 copy-start.1
  7.2 0.0 all-gather.3.cloned.1.call-start
  7.2 0.9 pad_maximum_fusion.2
  8.1 0.1 broadcast_in_dim.7
  8.2 0.0 copy-start.5
  8.2 0.0 copy-start.6
  8.2 25.7 %all_to_all.25 = bf16[8,32,1536]{2,1,0:T(8,128)(2,1)} all-to-all(bf16[8,32,1536]{2,1,0:T(8,128)(2,1)S(1)} %broadcast_in_dim.7), channel_id=1, replica_groups={{0,8,16,24,32,40,48,56},{1,65,129,193,257,321,385,449},{64,72,80,88,96,..., dimensions={0} | all-to-all | bytes 1572864 | tf_op jit(solution)/shard_map/all_to_all | solution.py:137
  33.9 0.0 all-gather.3.cloned.1.call-update
  34.0 0.0 copy-done.1
  34.0 1.3 copy.21
  35.3 0.8 dynamic_slice.14
  36.0 0.0 copy-done
  36.0 0.0 copy-done.5
  36.0 0.0 copy-done.6
  36.1 43.1 %all-gather.3.cloned.1.call-done = bf16[64,32,1536]{2,1,0:T(8,128)(2,1)} async-done(((bf16[8,32,1536]{2,1,0:T(8,128)(2,1)}), bf16[64,32,1536]{2,1,0:T(8,128)(2,1)}) %all-gather.3.cloned.1.call-update) | async-done | bytes 6291472 | tf_op jit(solution)/shard_map/all_gather | solution.py:141
  79.1 0.0 copy-start.2
  79.1 1.2 copy-done.2
  80.3 0.0 copy-start.3
  80.3 1.2 copy-done.3
  81.6 10.4 %layer.1 = (bf16[256,2048]{1,0:T(8,128)(2,1)S(1)}, bf16[256,2048]{1,0:T(8,128)(2,1)S(1)}, bf16[2048,512]{1,0:T(8,128)(2,1)}) custom-call(s32[2]{0:T(128)S(1)} %broadcast_select_fusion.2.stride_ref, bf16[256,2048]{1,0:T(8,128)(2,1)S(1)} %copy-done.2, bf16[256,2048]{1,0:T(8,128)(2,1)S(1)} %copy-done.3, bf16[256,2048]{1,0:T(8,128)(2,1)S(1)} %copy-done.1, ...), custom_call_target="tpu_custom_call" | custom-call | tf_op jit(solution)/shard_map/layer/pallas_call | solution.py:104
  92.0 1.1 fusion.2
  93.1 3.9 %collective-permute-start = (bf16[2,128,2048]{2,1,0:T(8,128)(2,1)}, bf16[2,128,2048]{2,1,0:T(8,128)(2,1)S(1)}, u32[]{:S(2)}, u32[]{:S(2)}) collective-permute-start(bf16[2,128,2048]{2,1,0:T(8,128)(2,1)} %fusion.2), channel_id=1, source_target_pairs={{0,1},{1,0},{2,3},{3,2},{4,5},{5,4},{6,7},{7,6},{8,9},{9,8},{10,11... | collective-permute-start | bytes 3145736 | tf_op jit(solution)/shard_map/ppermute | solution.py:124
  97.0 2.5 %collective-permute-done = bf16[2,128,2048]{2,1,0:T(8,128)(2,1)S(1)} collective-permute-done((bf16[2,128,2048]{2,1,0:T(8,128)(2,1)}, bf16[2,128,2048]{2,1,0:T(8,128)(2,1)S(1)}, u32[]{:S(2)}, u32[]{:S(2)}) %collective-permute-start) | collective-permute-done | bytes 1048608 | tf_op jit(solution)/shard_map/ppermute | solution.py:124
  99.5 0.4 fusion
  99.9 0.1 copy.24
  100.0 18.0 %all_to_all.26 = bf16[4,2,32,2048]{3,2,1,0:T(8,128)(2,1)S(1)} all-to-all(bf16[4,2,32,2048]{3,2,1,0:T(8,128)(2,1)S(1)} %copy.24), channel_id=1, replica_groups=mesh['z'=8,'y'=8,'x'=4,'c'=2] {'x'}, dimensions={0} | all-to-all | bytes 2097152 | tf_op jit(solution)/shard_map/all_to_all | solution.py:159
  118.0 0.2 reduce_sum.33
  118.2 0.1 broadcast_in_dim.8
  118.3 16.5 %all_to_all.27 = bf16[4,2,32,2048]{3,2,1,0:T(8,128)(2,1)} all-to-all(bf16[4,2,32,2048]{3,2,1,0:T(8,128)(2,1)S(1)} %broadcast_in_dim.8), channel_id=1, replica_groups=mesh['z'=8,'y'=8,'x'=4,'c'=2] {'x'}, dimensions={0} | all-to-all | bytes 2097152 | tf_op jit(solution)/shard_map/all_to_all | solution.py:160
  134.8 6.5 %all-to-all-start.3 = ((bf16[8,256,512]{2,1,0:T(8,128)(2,1)}), bf16[8,256,512]{2,1,0:T(8,128)(2,1)S(1)}, u32[]{:S(2)}, u32[]{:S(2)}) async-start(bf16[8,256,512]{2,1,0:T(8,128)(2,1)} %bitcast.46), calls=%async_computation.3 | async-start | bytes 4194304 | tf_op jit(solution)/shard_map/all_to_all | solution.py:147
  141.3 1.3 copy.25
  142.6 4.1 %collective-permute-start.1 = (bf16[2,128,2048]{2,1,0:T(8,128)(2,1)S(1)}, bf16[2,128,2048]{2,1,0:T(8,128)(2,1)}, u32[]{:S(2)}, u32[]{:S(2)}) collective-permute-start(bf16[2,128,2048]{2,1,0:T(8,128)(2,1)S(1)} %bitcast.44), channel_id=1, source_target_pairs={{0,1},{1,0},{2,3},{3,2},{4,5},{5,4},{6,7},{7,6},{8,9},{9,8},{10,11... | collective-permute-start | bytes 3145736 | tf_op jit(solution)/shard_map/ppermute | solution.py:124
  146.7 24.0 %all-to-all-done.3 = bf16[8,256,512]{2,1,0:T(8,128)(2,1)S(1)} async-done(((bf16[8,256,512]{2,1,0:T(8,128)(2,1)}), bf16[8,256,512]{2,1,0:T(8,128)(2,1)S(1)}, u32[]{:S(2)}, u32[]{:S(2)}) %all-to-all-start.3) | async-done | bytes 2097184 | tf_op jit(solution)/shard_map/all_to_all | solution.py:147
  170.7 1.1 reduce_sum.34
  171.7 3.8 %all-to-all-start.4 = ((bf16[8,32,512]{2,1,0:T(8,128)(2,1)}), bf16[8,32,512]{2,1,0:T(8,128)(2,1)S(1)}, u32[]{:S(2)}, u32[]{:S(2)}) async-start(bf16[8,32,512]{2,1,0:T(8,128)(2,1)} %bitcast.20), calls=%async_computation.4 | async-start | bytes 524288 | tf_op jit(solution)/shard_map/all_to_all | solution.py:151
  175.5 0.0 collective-permute-done.1
  175.6 1.4 broadcast_select_fusion.1
  176.9 0.2 slice_bitcast_fusion
  177.1 0.0 copy-start.4
  177.1 1.0 pad_maximum_fusion.1
  178.1 1.0 pad_maximum_fusion
  179.2 5.7 %all-to-all-done.4 = bf16[8,32,512]{2,1,0:T(8,128)(2,1)S(1)} async-done(((bf16[8,32,512]{2,1,0:T(8,128)(2,1)}), bf16[8,32,512]{2,1,0:T(8,128)(2,1)S(1)}, u32[]{:S(2)}, u32[]{:S(2)}) %all-to-all-start.4) | async-done | bytes 262176 | tf_op jit(solution)/shard_map/all_to_all | solution.py:151
  184.9 0.0 copy-done.4
  184.9 0.6 bitcast_add_fusion
  (3 shorter events, 0.0 us)
Async XLA Ops:
  7.2 28.9 %copy-start = (f32[3,4096]{1,0:T(4,128)S(1)}, f32[3,4096]{1,0:T(4,128)}, u32[]{:S(2)}) copy-start(f32[3,4096]{1,0:T(4,128)} %param.17) | copy-start | bytes 147460
  7.2 26.8 %copy-start.1 = (bf16[256,2048]{1,0:T(8,128)(2,1)S(1)}, bf16[256,2048]{1,0:T(8,128)(2,1)}, u32[]{:S(2)}) copy-start(bf16[256,2048]{1,0:T(8,128)(2,1)} %cot_ref.1) | copy-start | bytes 3145732
  7.2 71.9 %all-gather.3.cloned.1.call-start = ((), (), s32[]{:S(2)}) async-start(), calls=%async_computation.5 | async-start | bytes 7077888 | tf_op jit(solution)/shard_map/all_gather | solution.py:141
  8.2 27.9 %copy-start.5 = (s32[2]{0:T(128)S(1)}, s32[2]{0:T(128)}, u32[]{:S(2)}) copy-start(s32[2]{0:T(128)} %constant.35.clone) | copy-start | bytes 28
  8.2 27.8 %copy-start.6 = (s32[2]{0:T(128)S(1)}, s32[2]{0:T(128)}, u32[]{:S(2)}) copy-start(s32[2]{0:T(128)} %constant.36.clone) | copy-start | bytes 28
  79.1 1.2 copy-start.2
  80.3 1.2 copy-start.3
  93.1 6.4 %collective-permute-start = (bf16[2,128,2048]{2,1,0:T(8,128)(2,1)}, bf16[2,128,2048]{2,1,0:T(8,128)(2,1)S(1)}, u32[]{:S(2)}, u32[]{:S(2)}) collective-permute-start(bf16[2,128,2048]{2,1,0:T(8,128)(2,1)} %fusion.2), channel_id=1, source_target_pairs={{0,1},{1,0},{2,3},{3,2},{4,5},{5,4},{6,7},{7,6},{8,9},{9,8},{10,11... | collective-permute-start | bytes 3145736 | tf_op jit(solution)/shard_map/ppermute | solution.py:124
  134.8 35.8 %all-to-all-start.3 = ((bf16[8,256,512]{2,1,0:T(8,128)(2,1)}), bf16[8,256,512]{2,1,0:T(8,128)(2,1)S(1)}, u32[]{:S(2)}, u32[]{:S(2)}) async-start(bf16[8,256,512]{2,1,0:T(8,128)(2,1)} %bitcast.46), calls=%async_computation.3 | async-start | bytes 4194304 | tf_op jit(solution)/shard_map/all_to_all | solution.py:147
  142.6 32.9 %collective-permute-start.1 = (bf16[2,128,2048]{2,1,0:T(8,128)(2,1)S(1)}, bf16[2,128,2048]{2,1,0:T(8,128)(2,1)}, u32[]{:S(2)}, u32[]{:S(2)}) collective-permute-start(bf16[2,128,2048]{2,1,0:T(8,128)(2,1)S(1)} %bitcast.44), channel_id=1, source_target_pairs={{0,1},{1,0},{2,3},{3,2},{4,5},{5,4},{6,7},{7,6},{8,9},{9,8},{10,11... | collective-permute-start | bytes 3145736 | tf_op jit(solution)/shard_map/ppermute | solution.py:124
  171.7 13.1 %all-to-all-start.4 = ((bf16[8,32,512]{2,1,0:T(8,128)(2,1)}), bf16[8,32,512]{2,1,0:T(8,128)(2,1)S(1)}, u32[]{:S(2)}, u32[]{:S(2)}) async-start(bf16[8,32,512]{2,1,0:T(8,128)(2,1)} %bitcast.20), calls=%async_computation.4 | async-start | bytes 524288 | tf_op jit(solution)/shard_map/all_to_all | solution.py:151
  177.1 7.8 %copy-start.4 = (f32[512,32]{0,1:T(8,128)S(1)}, f32[512,32]{0,1:T(8,128)}, u32[]{:S(2)}) copy-start(f32[512,32]{0,1:T(8,128)} %param.19) | copy-start | bytes 196612
Sparse Core Ops, SparseCore 0:
  34.1 45.0 all-gather.2
